TPU v7x, 32 devices: a whole 2x2x4 slice. The times are simulated.
32 devices in a mesh: grp: 2 (over y), fs: 4 (over z), tp: 4 (over x, core).
Axes of the slice: x: 2, y: 2, z: 4, core: 2. Of those that a mesh axis runs over, the one named last changes fastest.
Arguments:
- tokens: bfloat16 [2048, 2048], P(('grp', 'fs')), parts along dimension 0, may hold values from -6 to 6
- ffn_pre_gain: bfloat16 [2048], replicated, may hold values from 0.099609375 to 1.8984375
- gate_weight: bfloat16 [2048, 5632], P('fs', 'tp'), may hold values from -0.125 to 0.125
- up_weight: bfloat16 [2048, 5632], P('fs', 'tp'), may hold values from -0.125 to 0.125
- down_weight: bfloat16 [5632, 2048], P('tp', 'fs'), may hold values from -0.078125 to 0.078125
- ffn_post_gain: bfloat16 [2048], replicated, may hold values from 0.099609375 to 1.8984375
- mix_pre_gain: bfloat16 [2048], replicated, may hold values from 0.099609375 to 1.8984375
- mix_u_weight: bfloat16 [2048, 2048], P('fs', 'tp'), may hold values from -0.125 to 0.125
- mix_v_weight: bfloat16 [2048, 2048], P('fs', 'tp'), may hold values from -0.125 to 0.125
- spatial_gain: bfloat16 [2048], P('tp'), may hold values from 0.099609375 to 1.8984375
- spatial_weight: bfloat16 [16, 128, 128], P('tp'), may hold values from -0.5 to 0.5
- spatial_bias: bfloat16 [16, 128], P('tp'), may hold values from 0.099609375 to 1.8984375
- mix_out_weight: bfloat16 [2048, 2048], P('tp', 'fs'), may hold values from -0.125 to 0.125
- mix_post_gain: bfloat16 [2048], replicated, may hold values from 0.099609375 to 1.8984375
- late_pre_gain: bfloat16 [2048], replicated, may hold values from 0.099609375 to 1.8984375
- late_post_gain: bfloat16 [2048], replicated, may hold values from 0.099609375 to 1.8984375
Outputs:
- result: bfloat16 [2048, 2048], P(('grp', 'fs')), parts along dimension 0
There are 2 independent parts, one for each index of `grp`. A program takes and returns all parts, laid end to end along the dimension named above; an argument that names none is the same for every part. Nothing has to cross between parts.
All inputs are finite; a program needn't handle non-finite values.
Results may differ from a plain program's by a relative error of at most 0.019.
Values may be sent and summed in bfloat16 or wider, within the bound.
A program may use at most 128 MiB of HBM per device.

v0:
```python
import jax
import jax.numpy as jnp
from jax import lax
from jax.sharding import PartitionSpec as P

GROUP_WIDTH = 128
BLOCK = 128


def row_norm(values, gain):
    scale = lax.rsqrt(jnp.mean(values * values, axis=-1, keepdims=True) + 1e-06)
    return values * scale * gain.astype(jnp.float32)


def reduce_partial(terms):
    return lax.psum(terms.astype(jnp.bfloat16), "tp").astype(jnp.float32)


def add_branch(stream, terms, gain, factor):
    total = reduce_partial(terms)
    return (stream.astype(jnp.float32) + factor * row_norm(total, gain)).astype(jnp.bfloat16)


def gated_hidden(normed, gate_full, up_full):
    gate = jnp.dot(normed, gate_full, preferred_element_type=jnp.float32)
    upper = jnp.dot(normed, up_full, preferred_element_type=jnp.float32)
    return (jax.nn.silu(gate) * upper).astype(jnp.bfloat16)


def spatial_mix(u_linear, v_linear, spatial_gain, spatial_weight, spatial_bias):
    count = u_linear.shape[0]
    gated_u = jax.nn.gelu(u_linear, approximate=False)
    gating_v = jax.nn.gelu(v_linear, approximate=False)
    groups = gating_v.shape[1] // GROUP_WIDTH
    grouped = gating_v.reshape(count, groups, GROUP_WIDTH)
    centred = grouped - jnp.mean(grouped, axis=-1, keepdims=True)
    vnorm = centred * lax.rsqrt(jnp.mean(centred * centred, axis=-1, keepdims=True) + 1e-05)
    vnorm = (vnorm * spatial_gain.astype(jnp.float32).reshape(groups, GROUP_WIDTH)).astype(
        jnp.bfloat16
    )
    blocks = vnorm.reshape(count // BLOCK, BLOCK, groups, GROUP_WIDTH)
    lower = jnp.tril(jnp.ones((BLOCK, BLOCK), dtype=bool))
    masked = jnp.where(lower[None], spatial_weight, jnp.zeros_like(spatial_weight))
    spatial = jnp.einsum("gts,nsgc->ntgc", masked, blocks, preferred_element_type=jnp.float32)
    spatial = spatial + spatial_bias.astype(jnp.float32).T[None, :, :, None]
    return (gated_u * spatial.reshape(count, groups * GROUP_WIDTH)).astype(jnp.bfloat16)


def shards(
    tokens,
    ffn_pre_gain,
    gate_weight,
    up_weight,
    down_weight,
    ffn_post_gain,
    mix_pre_gain,
    mix_u_weight,
    mix_v_weight,
    spatial_gain,
    spatial_weight,
    spatial_bias,
    mix_out_weight,
    mix_post_gain,
    late_pre_gain,
    late_post_gain,
):
    normed = row_norm(tokens.astype(jnp.float32), ffn_pre_gain).astype(jnp.bfloat16)
    gate_full, up_full = (
        lax.all_gather(gate_weight, "fs", axis=0, tiled=True),
        lax.all_gather(up_weight, "fs", axis=0, tiled=True),
    )
    down_full = lax.all_gather(down_weight, "fs", axis=1, tiled=True)
    hidden = gated_hidden(normed, gate_full, up_full)
    terms = jnp.dot(hidden, down_full, preferred_element_type=jnp.float32)
    first = add_branch(tokens, terms, ffn_post_gain, 0.5)
    normed = row_norm(first.astype(jnp.float32), mix_pre_gain).astype(jnp.bfloat16)
    u_full, v_full = (
        lax.all_gather(mix_u_weight, "fs", axis=0, tiled=True),
        lax.all_gather(mix_v_weight, "fs", axis=0, tiled=True),
    )
    u_linear = jnp.dot(normed, u_full, preferred_element_type=jnp.float32)
    v_linear = jnp.dot(normed, v_full, preferred_element_type=jnp.float32)
    mixed = spatial_mix(u_linear, v_linear, spatial_gain, spatial_weight, spatial_bias)
    out_full = lax.all_gather(mix_out_weight, "fs", axis=1, tiled=True)
    terms = jnp.dot(mixed, out_full, preferred_element_type=jnp.float32)
    second = add_branch(first, terms, mix_post_gain, 1.0)
    normed = row_norm(second.astype(jnp.float32), late_pre_gain).astype(jnp.bfloat16)
    hidden = gated_hidden(normed, gate_full, up_full)
    terms = jnp.dot(hidden, down_full, preferred_element_type=jnp.float32)
    return add_branch(second, terms, late_post_gain, 0.5)


def solution(mesh):
    in_specs = (
        P(("grp", "fs"), None),
        P(),
        P("fs", "tp"),
        P("fs", "tp"),
        P("tp", "fs"),
        P(),
        P(),
        P("fs", "tp"),
        P("fs", "tp"),
        P("tp"),
        P("tp", None, None),
        P("tp", None),
        P("tp", "fs"),
        P(),
        P(),
        P(),
    )
    out_specs = P(("grp", "fs"), None)
    return jax.shard_map(shards, mesh=mesh, in_specs=in_specs, out_specs=out_specs, check_vma=False)
```

profile of v0, /device:TPU:1, one launch (start us, length us, event | category | flops | bytes accessed | tf_op | source)
XLA Modules:
  0.0 619.2 jit_solution(5151979985591970159)
XLA Ops:
  6.5 0.7 all-gather.7.cloned.1.call-update
  7.3 0.0 all-gather.11.cloned.1.call-start
  7.3 0.7 all-gather.11.cloned.1.call-update
  8.0 0.0 all-gather.9.cloned.1.call-start
  8.1 0.7 all-gather.9.cloned.1.call-update
  8.7 0.0 all-reduce.4.cloned.1.call-start
  8.8 0.3 fusion.10
  9.1 108.7 %all-gather.7.cloned.1.call-done = bf16[2048,1408]{1,0:T(8,128)(2,1)} async-done(((bf16[512,1408]{1,0:T(8,128)(2,1)}), bf16[2048,1408]{1,0:T(8,128)(2,1)}) %all-gather.7.cloned.1.call-update) | async-done | bytes 5767184 | tf_op jit(solution)/shard_map/all_gather | solution.py:69
  117.8 4.5 fusion.59
  122.3 102.1 %all-gather.11.cloned.1.call-done = bf16[1408,2048]{1,0:T(8,128)(2,1)} async-done(((bf16[1408,512]{1,0:T(8,128)(2,1)}), bf16[1408,2048]{1,0:T(8,128)(2,1)}) %all-gather.11.cloned.1.call-update) | async-done | bytes 5767184 | tf_op jit(solution)/shard_map/all_gather | solution.py:72
  224.3 106.6 %all-gather.9.cloned.1.call-done = bf16[2048,1408]{1,0:T(8,128)(2,1)} async-done(((bf16[512,1408]{1,0:T(8,128)(2,1)}), bf16[2048,1408]{1,0:T(8,128)(2,1)}) %all-gather.9.cloned.1.call-update) | async-done | bytes 5767184 | tf_op jit(solution)/shard_map/all_gather | solution.py:70
  330.9 8.9 %convolution_convert_fusion.2 = bf16[256,2048]{1,0:T(8,128)(2,1)} fusion(bf16[1408,2048]{1,0:T(8,128)(2,1)} %all-gather.11.cloned.1.call-done, bf16[2048,1408]{1,0:T(8,128)(2,1)} %all-gather.9.cloned.1.call-done, f32[256,1408]{1,0:T(8,128)S(1)} %fusion.59, bf16[256,2048]{1,0:T(8,128)(2,1)S(1)} %copy-done, f32[2048]{0:T(1024)S(1)} %convert_element_type.82, ...), kind=kOutput, calls=%fused_computation.21 | convolution fusion | flops 2957574144 | bytes 15082496 | tf_op jit(solution)/shard_map/dot_general | solution.py:74
  339.8 0.0 all-reduce.4.cloned.1.call-update
  339.8 0.0 all-gather.15.cloned.1.call-start
  339.9 0.5 all-gather.15.cloned.1.call-update
  340.4 0.0 all-gather.13.cloned.1.call-start
  340.5 0.5 all-gather.13.cloned.1.call-update
  341.0 0.0 all-gather.17.cloned.1.call-start
  341.1 0.7 all-gather.17.cloned.1.call-update
  341.8 0.2 all-reduce.6.cloned.1.call-start
  342.1 32.0 %all-reduce.4.cloned.1.call-done = bf16[256,2048]{1,0:T(8,128)(2,1)} async-done(((bf16[256,2048]{1,0:T(8,128)(2,1)}), bf16[256,2048]{1,0:T(8,128)(2,1)}) %all-reduce.4.cloned.1.call-update) | async-done | bytes 1048592 | tf_op jit(solution)/shard_map/psum | solution.py:16
  374.1 1.5 fusion.2
  375.6 1.9 fusion.14
  377.6 44.3 %all-gather.15.cloned.1.call-done = bf16[2048,512]{1,0:T(8,128)(2,1)} async-done(((bf16[512,512]{1,0:T(8,128)(2,1)}), bf16[2048,512]{1,0:T(8,128)(2,1)}) %all-gather.15.cloned.1.call-update) | async-done | bytes 2097168 | tf_op jit(solution)/shard_map/all_gather | solution.py:79
  421.9 3.4 fusion.28
  425.2 0.2 reshape.99
  425.4 0.2 reshape.98
  425.6 0.3 reduce_sum.75
  426.0 0.6 multiply_reduce_fusion
  426.7 0.1 copy.36
  426.8 0.1 copy.37
  426.8 0.2 copy.25
  427.1 0.3 fusion.22
  427.4 0.2 copy.28
  427.6 40.1 %all-gather.13.cloned.1.call-done = bf16[2048,512]{1,0:T(8,128)(2,1)} async-done(((bf16[512,512]{1,0:T(8,128)(2,1)}), bf16[2048,512]{1,0:T(8,128)(2,1)}) %all-gather.13.cloned.1.call-update) | async-done | bytes 2097168 | tf_op jit(solution)/shard_map/all_gather | solution.py:78
  467.8 46.1 %all-gather.17.cloned.1.call-done = bf16[512,2048]{1,0:T(8,128)(2,1)} async-done(((bf16[512,512]{1,0:T(8,128)(2,1)}), bf16[512,2048]{1,0:T(8,128)(2,1)}) %all-gather.17.cloned.1.call-update) | async-done | bytes 2097168 | tf_op jit(solution)/shard_map/all_gather | solution.py:84
  513.8 5.7 convolution_convert_fusion
  519.6 0.0 all-reduce.6.cloned.1.call-update
  519.6 0.3 all-reduce.8.cloned.1.call-start
  519.9 34.8 %all-reduce.6.cloned.1.call-done = bf16[256,2048]{1,0:T(8,128)(2,1)} async-done(((bf16[256,2048]{1,0:T(8,128)(2,1)}), bf16[256,2048]{1,0:T(8,128)(2,1)}) %all-reduce.6.cloned.1.call-update) | async-done | bytes 1048592 | tf_op jit(solution)/shard_map/psum | solution.py:16
  554.7 1.5 fusion.5
  556.2 1.9 fusion.18
  558.1 4.5 fusion.45
  562.6 8.9 %convolution_convert_fusion.1 = bf16[256,2048]{1,0:T(8,128)(2,1)} fusion(bf16[1408,2048]{1,0:T(8,128)(2,1)} %all-gather.11.cloned.1.call-done, bf16[2048,1408]{1,0:T(8,128)(2,1)} %all-gather.9.cloned.1.call-done, f32[256,1408]{1,0:T(8,128)S(1)} %fusion.45, bf16[256,2048]{1,0:T(8,128)(2,1)S(1)} %get-tuple-element.6, f32[2048]{0:T(1024)S(1)} %convert_element_type.99, ...), kind=kOutput, calls=%fused_computation.20 | convolution fusion | flops 2957574144 | bytes 15082496 | tf_op jit(solution)/shard_map/dot_general | solution.py:89
  571.5 0.0 all-reduce.8.cloned.1.call-update
  571.5 36.9 %all-reduce.8.cloned.1.call-done = bf16[256,2048]{1,0:T(8,128)(2,1)} async-done(((bf16[256,2048]{1,0:T(8,128)(2,1)}), bf16[256,2048]{1,0:T(8,128)(2,1)}) %all-reduce.8.cloned.1.call-update) | async-done | bytes 1048592 | tf_op jit(solution)/shard_map/psum | solution.py:16
  608.4 1.5 fusion.7
  609.9 2.8 fusion.21
  (38 shorter events, 0.2 us)
Async XLA Ops:
  6.5 2.3 copy-start.2
  6.5 2.3 copy-start
  6.5 111.2 %all-gather.7.cloned.1.call-start = ((), (), s32[]{:S(2)}) async-start(), calls=%async_computation | async-start | bytes 7208960 | tf_op jit(solution)/shard_map/all_gather | solution.py:69
  7.3 217.1 %all-gather.11.cloned.1.call-start = ((), (), s32[]{:S(2)}) async-start(), calls=%async_computation.2 | async-start | bytes 7208960 | tf_op jit(solution)/shard_map/all_gather | solution.py:72
  8.0 322.9 %all-gather.9.cloned.1.call-start = ((), (), s32[]{:S(2)}) async-start(), calls=%async_computation.1 | async-start | bytes 7208960 | tf_op jit(solution)/shard_map/all_gather | solution.py:70
  8.7 365.4 %all-reduce.4.cloned.1.call-start = ((), (), s32[]{:S(2)}) async-start(), calls=%async_computation.3 | async-start | bytes 2097152 | tf_op jit(solution)/shard_map/psum | solution.py:16
  339.8 2.2 copy-start.3
  339.8 2.2 copy-start.4
  339.8 2.2 copy-start.8
  339.8 2.3 copy-start.9
  339.8 82.0 %all-gather.15.cloned.1.call-start = ((), (), s32[]{:S(2)}) async-start(), calls=%async_computation.5 | async-start | bytes 2621440 | tf_op jit(solution)/shard_map/all_gather | solution.py:79
  340.4 127.3 %all-gather.13.cloned.1.call-start = ((), (), s32[]{:S(2)}) async-start(), calls=%async_computation.4 | async-start | bytes 2621440 | tf_op jit(solution)/shard_map/all_gather | solution.py:78
  341.0 172.8 %all-gather.17.cloned.1.call-start = ((), (), s32[]{:S(2)}) async-start(), calls=%async_computation.6 | async-start | bytes 2621440 | tf_op jit(solution)/shard_map/all_gather | solution.py:84
  341.8 212.9 %all-reduce.6.cloned.1.call-start = ((), (), s32[]{:S(2)}) async-start(), calls=%async_computation.7 | async-start | bytes 2097152 | tf_op jit(solution)/shard_map/psum | solution.py:16
  425.4 1.7 copy-start.1
  513.8 6.0 copy-start.5
  513.8 6.0 copy-start.6
  519.6 88.8 %all-reduce.8.cloned.1.call-start = ((), (), s32[]{:S(2)}) async-start(), calls=%async_computation.8 | async-start | bytes 2097152 | tf_op jit(solution)/shard_map/psum | solution.py:16
  562.6 9.0 %copy-start.7 = (bf16[2048]{0:T(1024)(128)(2,1)S(1)}, bf16[2048]{0:T(1024)(128)(2,1)}, u32[]{:S(2)}) copy-start(bf16[2048]{0:T(1024)(128)(2,1)} %param.31) | copy-start | bytes 12292
Sparse Core Ops, SparseCore 0:
  8.9 108.8 all-gather.6
  119.4 104.9 all-gather.10
  225.9 104.9 all-gather.8
  340.0 34.0 all-reduce.3
  375.5 46.2 all-gather.14
  423.3 44.4 all-gather.12
  469.3 44.4 all-gather.16
  519.7 34.9 all-reduce.5
  571.6 36.7 all-reduce.7
where the time goes:
time: 621 us; the launch traced here: 619 us
  waiting for transfers between devices  555 us (89%)
  matrix products  36.2 us (6%)
  between operations  13.5 us (2%)
  other arithmetic  12.5 us (2%)
    all_gather x1, waiting for transfers between devices, shards(): lax.all_gather(gate_weight, 'fs', axis=0, tiled=True)  109 us
    all_gather x1, waiting for transfers between devices, shards(): lax.all_gather(up_weight, 'fs', axis=0, tiled=True)  107 us
    psum x3, waiting for transfers between devices, reduce_partial(): return lax.psum(terms.astype(jnp.bfloat16), 'tp').astype(jnp.float32)  104 us
    all_gather x1, waiting for transfers between devices, shards(): down_full = lax.all_gather(down_weight, 'fs', axis=1, tiled=True)  102 us
    all_gather x1, waiting for transfers between devices, shards(): out_full = lax.all_gather(mix_out_weight, 'fs', axis=1, tiled=True)  46.1 us
    all_gather x1, waiting for transfers between devices, shards(): lax.all_gather(mix_v_weight, 'fs', axis=0, tiled=True)  44.3 us
    all_gather x1, waiting for transfers between devices, shards(): lax.all_gather(mix_u_weight, 'fs', axis=0, tiled=True)  40.1 us
    dot_general x2, matrix products, shards(): terms = jnp.dot(hidden, down_full, preferred_element_type=jnp.float32)  17.8 us
  transfers between devices with their start and end apart: 9, of which 9 were waited for; matrix products, arithmetic and copies ran while one was open for 2% of the time, Pallas kernels for 0%

commit v1 on v0

v1 whole, which is shorter than its diff:
```python
import functools

import jax
import jax.numpy as jnp
from jax import lax
from jax.experimental import pallas as pl
from jax.experimental.pallas import tpu as pltpu
from jax.sharding import PartitionSpec as P

GROUP_WIDTH = 128
BLOCK = 128
TILE = 256
F32 = jnp.float32
BF16 = jnp.bfloat16
MESH = pl.DeviceIdType.MESH
SPLITS = (2, 2, 2, 1, 1, 1)


def aligned(value, unit):
    return value if isinstance(value, int) else pl.multiple_of(value, unit)


def over_tiles(width, body):
    count = width // TILE

    def step(i, carry):
        body(pl.multiple_of(i * TILE, TILE), TILE)
        return carry

    lax.fori_loop(0, count, step, 0)
    if width % TILE:
        body(count * TILE, width % TILE)


def over_rows(count, size, body):
    def step(i, carry):
        body(pl.multiple_of(i * size, size))
        return carry

    lax.fori_loop(0, count // size, step, 0)


def gelu(a):
    return 0.5 * a * (1.0 + lax.erf(a * (2.0**-0.5)))


def kernel(
    sizes,
    tokens,
    gains,
    gate_w,
    up_w,
    down_w,
    u_w,
    v_w,
    out_w,
    spatial_gain,
    spatial_weight,
    spatial_bias,
    result,
    gate_full,
    up_full,
    down_full,
    u_full,
    v_full,
    out_full,
    normed,
    hidden,
    mixed,
    parts,
    landed,
    streams,
    own_sem,
    left_send,
    left_recv,
    right_send,
    right_recv,
    side_send,
    side_recv,
    sum_send,
    sum_recv,
    put_send,
    put_recv,
    last_sem,
):
    grp_n, fs_n, tp_n = sizes
    grp, fs, tp = lax.axis_index("grp"), lax.axis_index("fs"), lax.axis_index("tp")
    shards = (gate_w, up_w, down_w, u_w, v_w, out_w)
    fulls = (gate_full, up_full, down_full, u_full, v_full, out_full)
    count, width = tokens.shape
    chunk = count // tp_n

    barrier = pltpu.get_barrier_semaphore()
    for move in (1, fs_n - 1):
        pl.semaphore_signal(
            barrier, inc=1, device_id={"fs": lax.rem(fs + move, fs_n)}, device_id_type=MESH
        )
    for move in range(1, grp_n):
        pl.semaphore_signal(
            barrier, inc=1, device_id={"grp": lax.rem(grp + move, grp_n)}, device_id_type=MESH
        )
    for move in range(1, tp_n):
        pl.semaphore_signal(
            barrier, inc=1, device_id={"tp": lax.rem(tp + move, tp_n)}, device_id_type=MESH
        )
    pl.semaphore_wait(barrier, 2 + grp_n - 1 + tp_n - 1)

    units = []
    for w in range(6):
        piece = shards[w].shape[0] // grp_n // SPLITS[w]
        for s in range(SPLITS[w]):
            units.append((w, s * piece, piece))

    def unit_rows(unit):
        w, low, piece = units[unit]
        return aligned(grp * (shards[w].shape[0] // grp_n) + low, 16), piece

    def place(w, block, low, piece):
        if w in (2, 5):
            return fulls[w].at[block, pl.ds(low, piece), :]
        start = aligned(block * shards[w].shape[0] + low, 16)
        return fulls[w].at[pl.ds(start, piece), :]

    def own_copy(w):
        return pltpu.make_async_copy(
            shards[w], place(w, fs, 0, shards[w].shape[0]), own_sem.at[w]
        )

    def to_right(unit, hop, own=False):
        w = units[unit][0]
        low, piece = unit_rows(unit)
        target = place(w, fs - hop, low, piece)
        source = shards[w].at[pl.ds(low, piece), :] if own else target
        return pltpu.make_async_remote_copy(
            src_ref=source,
            dst_ref=target,
            send_sem=right_send.at[unit, hop],
            recv_sem=right_recv.at[unit, hop],
            device_id={"fs": fs + 1},
            device_id_type=MESH,
        )

    def to_left(unit, hop, own=False):
        w = units[unit][0]
        low, piece = unit_rows(unit)
        target = place(w, fs + hop, low, piece)
        source = shards[w].at[pl.ds(low, piece), :] if own else target
        return pltpu.make_async_remote_copy(
            src_ref=source,
            dst_ref=target,
            send_sem=left_send.at[unit, hop],
            recv_sem=left_recv.at[unit, hop],
            device_id={"fs": fs - 1},
            device_id_type=MESH,
        )

    def to_side(unit, side, hop, move):
        w = units[unit][0]
        low, piece = unit_rows(unit)
        block = fs - hop if side == 0 else fs + hop
        target = place(w, block, low, piece)
        return pltpu.make_async_remote_copy(
            src_ref=target,
            dst_ref=target,
            send_sem=side_send.at[unit, side, move - 1, hop],
            recv_sem=side_recv.at[unit, side, move - 1, hop],
            device_id={"grp": lax.rem(grp + move, grp_n)},
            device_id_type=MESH,
        )

    def send_own(unit):
        if unit >= len(units):
            return

        @pl.when(fs < fs_n - 1)
        def _():
            to_right(unit, 0, own=True).start()

        @pl.when(fs > 0)
        def _():
            to_left(unit, 0, own=True).start()

    def relay(unit):
        def step(hop, carry):
            @pl.when(fs >= hop)
            def _():
                to_right(unit, hop - 1).wait_recv()

                @pl.when(fs < fs_n - 1)
                def _():
                    to_right(unit, hop).start()

                for move in range(1, grp_n):
                    to_side(unit, 0, hop, move).start()

            @pl.when(fs + hop < fs_n)
            def _():
                to_left(unit, hop - 1).wait_recv()

                @pl.when(fs > 0)
                def _():
                    to_left(unit, hop).start()

                for move in range(1, grp_n):
                    to_side(unit, 1, hop, move).start()

            return carry

        lax.fori_loop(1, fs_n, step, 0)

    def wait_weight(w):
        own_copy(w).wait()
        for unit in range(len(units)):
            if units[unit][0] == w:

                def step(hop, carry, unit=unit):
                    for move in range(1, grp_n):

                        @pl.when(fs >= hop)
                        def _():
                            to_side(unit, 0, hop, move).wait_recv()

                        @pl.when(fs + hop < fs_n)
                        def _():
                            to_side(unit, 1, hop, move).wait_recv()

                    return carry

                lax.fori_loop(1, fs_n, step, 0)

    def finish_sends():
        for unit in range(len(units)):

            def step(hop, carry, unit=unit):
                @pl.when((fs >= hop) & (fs < fs_n - 1))
                def _():
                    to_right(unit, hop).wait_send()

                @pl.when((fs + hop < fs_n) & (fs > 0))
                def _():
                    to_left(unit, hop).wait_send()

                @pl.when(hop > 0)
                def _():
                    for move in range(1, grp_n):

                        @pl.when(fs >= hop)
                        def _():
                            to_side(unit, 0, hop, move).wait_send()

                        @pl.when(fs + hop < fs_n)
                        def _():
                            to_side(unit, 1, hop, move).wait_send()

                return carry

            lax.fori_loop(0, fs_n, step, 0)

    def sum_copy(phase, move):
        peer = lax.rem(tp + move, tp_n)
        rows = pl.ds(aligned(peer * chunk, 16), chunk)
        return pltpu.make_async_remote_copy(
            src_ref=parts.at[phase, rows, :],
            dst_ref=landed.at[phase, move - 1],
            send_sem=sum_send.at[phase, move - 1],
            recv_sem=sum_recv.at[phase, move - 1],
            device_id={"tp": peer},
            device_id_type=MESH,
        )

    def put_copy(phase, move):
        rows = pl.ds(aligned(tp * chunk, 16), chunk)
        return pltpu.make_async_remote_copy(
            src_ref=streams.at[phase, rows, :],
            dst_ref=streams.at[phase, rows, :],
            send_sem=put_send.at[phase, move - 1],
            recv_sem=put_recv.at[phase, move - 1],
            device_id={"tp": lax.rem(tp + move, tp_n)},
            device_id_type=MESH,
        )

    def gain(row):
        return gains[row : row + 1, :].astype(F32)

    def norm_rows(load, row):
        def body(low):
            values = load(pl.ds(low, 32)).astype(F32)
            scale = lax.rsqrt(jnp.mean(values * values, axis=-1, keepdims=True) + 1e-06)
            normed[pl.ds(low, 32), :] = (values * scale * gain(row)).astype(BF16)

        over_rows(count, 32, body)

    def start_sums(phase):
        for move in range(1, tp_n):
            sum_copy(phase, move).start()

    def add_branch(phase, load, row, factor):
        for move in range(1, tp_n):
            sum_copy(phase, move).wait_recv()

        def body(low):
            rows = pl.ds(aligned(tp * chunk + low, 16), 16)
            total = parts[phase, rows, :].astype(F32)
            for move in range(1, tp_n):
                total = total + landed[phase, move - 1, pl.ds(low, 16), :].astype(F32)
            scale = lax.rsqrt(jnp.mean(total * total, axis=-1, keepdims=True) + 1e-06)
            branch = total * scale * gain(row)
            streams[phase, rows, :] = (load(rows).astype(F32) + factor * branch).astype(BF16)

        over_rows(chunk, 16, body)
        for move in range(1, tp_n):
            put_copy(phase, move).start()

    def wait_put(phase):
        for move in range(1, tp_n):
            put_copy(phase, move).wait_recv()

    def hidden_units():
        def body(low, size):
            cols = pl.ds(low, size)
            gate = jnp.dot(normed[...], gate_full[:, cols], preferred_element_type=F32)
            upper = jnp.dot(normed[...], up_full[:, cols], preferred_element_type=F32)
            hidden[:, cols] = (gate / (1.0 + jnp.exp(-gate)) * upper).astype(BF16)

        over_tiles(hidden.shape[1], body)

    def project(phase, left, right):
        size = right.shape[2]

        def one(block, low):
            terms = jnp.dot(left[...], right[block], preferred_element_type=F32)
            parts[phase, :, pl.ds(low, size)] = terms.astype(BF16)

        if size % 128 == 0:

            def step(block, carry):
                one(block, pl.multiple_of(block * size, 128))
                return carry

            lax.fori_loop(0, fs_n, step, 0)
        else:
            for block in range(fs_n):
                one(block, block * size)

    def mix():
        rows = lax.broadcasted_iota(jnp.int32, (BLOCK, BLOCK), 0)
        cols = lax.broadcasted_iota(jnp.int32, (BLOCK, BLOCK), 1)
        for g in range(mixed.shape[1] // GROUP_WIDTH):
            span = slice(g * GROUP_WIDTH, (g + 1) * GROUP_WIDTH)
            v = gelu(jnp.dot(normed[...], v_full[:, span], preferred_element_type=F32))
            u = gelu(jnp.dot(normed[...], u_full[:, span], preferred_element_type=F32))
            v = v - jnp.mean(v, axis=-1, keepdims=True)
            v = v * lax.rsqrt(jnp.mean(v * v, axis=-1, keepdims=True) + 1e-05)
            v = (v * spatial_gain[:, span].astype(F32)).astype(BF16)
            weight = spatial_weight[g].astype(F32)
            weight = jnp.where(rows >= cols, weight, 0.0).astype(BF16)
            for n in range(count // BLOCK):
                part = slice(n * BLOCK, (n + 1) * BLOCK)
                spatial = jnp.dot(weight, v[part], preferred_element_type=F32)
                spatial = spatial + spatial_bias[:, g : g + 1]
                mixed[part, span] = (u[part] * spatial).astype(BF16)

    load_tokens = lambda rows: tokens[rows, :]
    load_first = lambda rows: streams[0, rows, :]
    load_second = lambda rows: streams[1, rows, :]

    send_own(0)
    send_own(1)
    for w in range(6):
        own_copy(w).start()
    norm_rows(load_tokens, 0)

    def relay_weight(w):
        for unit in range(len(units)):
            if units[unit][0] == w:
                relay(unit)
                send_own(unit + 2)

    relay_weight(0)
    relay_weight(1)
    wait_weight(0)
    relay_weight(2)
    wait_weight(1)
    hidden_units()
    wait_weight(2)
    project(0, hidden, down_full)
    start_sums(0)
    relay_weight(3)
    add_branch(0, load_tokens, 1, 0.5)
    relay_weight(4)
    wait_put(0)
    norm_rows(load_first, 2)
    relay_weight(5)
    wait_weight(3)
    wait_weight(4)
    mix()
    wait_weight(5)
    project(1, mixed, out_full)
    start_sums(1)
    add_branch(1, load_first, 3, 1.0)
    wait_put(1)
    norm_rows(load_second, 4)
    hidden_units()
    project(2, hidden, down_full)
    start_sums(2)
    add_branch(2, load_second, 5, 0.5)
    finish_sends()
    wait_put(2)
    last = pltpu.make_async_copy(streams.at[2], result, last_sem)
    last.start()
    for phase in range(3):
        for move in range(1, tp_n):
            sum_copy(phase, move).wait_send()
            put_copy(phase, move).wait_send()
    last.wait()


def shards(
    sizes,
    tokens,
    ffn_pre_gain,
    gate_weight,
    up_weight,
    down_weight,
    ffn_post_gain,
    mix_pre_gain,
    mix_u_weight,
    mix_v_weight,
    spatial_gain,
    spatial_weight,
    spatial_bias,
    mix_out_weight,
    mix_post_gain,
    late_pre_gain,
    late_post_gain,
):
    grp_n, fs_n, tp_n = sizes
    count, width = tokens.shape
    hidden_width = gate_weight.shape[1]
    channels = mix_u_weight.shape[1]
    gains = jnp.stack(
        [ffn_pre_gain, ffn_post_gain, mix_pre_gain, mix_post_gain, late_pre_gain, late_post_gain]
    )
    vmem = pl.BlockSpec(memory_space=pltpu.VMEM)
    hbm = pl.BlockSpec(memory_space=pl.ANY)
    units = sum(SPLITS)
    dma = pltpu.SemaphoreType.DMA
    return pl.pallas_call(
        functools.partial(kernel, sizes),
        out_shape=jax.ShapeDtypeStruct((count, width), BF16),
        in_specs=[vmem, vmem, hbm, hbm, hbm, hbm, hbm, hbm, vmem, vmem, vmem],
        out_specs=hbm,
        scratch_shapes=[
            pltpu.VMEM((width, hidden_width), BF16),
            pltpu.VMEM((width, hidden_width), BF16),
            pltpu.VMEM((fs_n,) + down_weight.shape, BF16),
            pltpu.VMEM((width, channels), BF16),
            pltpu.VMEM((width, channels), BF16),
            pltpu.VMEM((fs_n,) + mix_out_weight.shape, BF16),
            pltpu.VMEM((count, width), BF16),
            pltpu.VMEM((count, hidden_width), BF16),
            pltpu.VMEM((count, channels), BF16),
            pltpu.VMEM((3, count, width), BF16),
            pltpu.VMEM((3, tp_n - 1, count // tp_n, width), BF16),
            pltpu.VMEM((3, count, width), BF16),
            dma((6,)),
            dma((units, fs_n)),
            dma((units, fs_n)),
            dma((units, fs_n)),
            dma((units, fs_n)),
            dma((units, 2, grp_n - 1, fs_n)),
            dma((units, 2, grp_n - 1, fs_n)),
            dma((3, tp_n - 1)),
            dma((3, tp_n - 1)),
            dma((3, tp_n - 1)),
            dma((3, tp_n - 1)),
            dma(()),
        ],
        compiler_params=pltpu.CompilerParams(
            collective_id=0, has_side_effects=True, vmem_limit_bytes=60 * 2**20
        ),
    )(
        tokens,
        gains,
        gate_weight,
        up_weight,
        down_weight,
        mix_u_weight,
        mix_v_weight,
        mix_out_weight,
        spatial_gain.reshape(1, channels),
        spatial_weight,
        spatial_bias.astype(F32).T,
    )


def solution(mesh):
    in_specs = (
        P(("grp", "fs"), None),
        P(),
        P("fs", "tp"),
        P("fs", "tp"),
        P("tp", "fs"),
        P(),
        P(),
        P("fs", "tp"),
        P("fs", "tp"),
        P("tp"),
        P("tp", None, None),
        P("tp", None),
        P("tp", "fs"),
        P(),
        P(),
        P(),
    )
    out_specs = P(("grp", "fs"), None)
    sizes = (mesh.shape["grp"], mesh.shape["fs"], mesh.shape["tp"])
    body = functools.partial(shards, sizes)
    return jax.shard_map(body, mesh=mesh, in_specs=in_specs, out_specs=out_specs, check_vma=False)
```

time: 621 us -> 283 us (0.46)
  waiting for transfers between devices: 555 us -> 0 us
  Pallas kernels: 0 us -> 273 us
  matrix products: 36.2 us -> 0 us
  between operations: 13.5 us -> 0.01 us
  other arithmetic: 12.5 us -> 0 us
  local copies, waits for them, and re-layouts: 1.03 us -> 9.8 us
    all_gather x6 -> x0, waiting for transfers between devices: 448 us -> none  [the longest x1 109 us: shards(): lax.all_gather(gate_weight, 'fs', axis=0, tiled=True)]
    pallas_call x0 -> x1, Pallas kernels: none -> 273 us  [shards(): pl.pallas_call(functools.partial(kernel, sizes), out_shape=jax.ShapeDtype...]
    psum x3 -> x0, waiting for transfers between devices: 104 us -> none  [reduce_partial(): return lax.psum(terms.astype(jnp.bfloat16), 'tp').astype(jnp.float32)]
    dot_general x7 -> x0, matrix products: 36.2 us -> none  [the longest x2 17.8 us: shards(): terms = jnp.dot(hidden, down_full, preferred_element_type=jnp.float32)]
    reduce_sum x8 -> x0, other arithmetic: 9.63 us -> none  [the longest x6 8.65 us: row_norm(): scale = lax.rsqrt(jnp.mean(values * values, axis=-1, keepdims=True) + 1e-06)]
  transfers between devices with their start and end apart: 9 -> 0, of which waited for: 9 -> 0; matrix products, arithmetic and copies ran while one was open for 2% -> 0% of each run, Pallas kernels for 0% -> 0%
where the time goes in v1:
time: 283 us
  Pallas kernels  273 us (96%)
  local copies, waits for them, and re-layouts  9.8 us (3%)
    pallas_call x1, Pallas kernels, shards(): pl.pallas_call(functools.partial(kernel, sizes), out_shape=jax.ShapeDtype...  273 us

profile of v1, /device:TPU:1, one launch (start us, length us, event | category | flops | bytes accessed | tf_op | source)
XLA Modules:
  0.0 282.7 jit_solution(1214562146362490048)
XLA Ops:
  0.0 1.2 reshape.3.spatial_gain
  1.2 0.7 stack.21
  1.9 0.7 stack.22
  2.6 0.7 stack.23
  3.3 0.7 stack.24
  4.0 0.7 stack.25
  4.7 0.7 stack.26
  5.4 0.7 stack.27.gains
  6.1 1.4 copy.17
  7.5 272.8 %shard_map.154 = bf16[256,2048]{1,0:T(8,128)(2,1)} custom-call(bf16[256,2048]{1,0:T(8,128)(2,1)} %tokens.1, bf16[6,2048]{1,0:T(8,128)(2,1)} %stack.27.gains, bf16[512,1408]{1,0:T(8,128)(2,1)} %gate_w.1, bf16[512,1408]{1,0:T(8,128)(2,1)} %up_w.1, bf16[1408,512]{1,0:T(8,128)(2,1)} %down_w.1, bf16[512,512]{1,0:T(8,128)(2,1)} %u_w.1, bf16[512,512]{1,0:T(8,128)(2,1)} %v_w.1, ...), custom_call_target="tpu_custom_call" | custom-call | tf_op jit(solution)/shard_map/pallas_call | solution.py:448
  280.4 2.3 copy.19

commit v2 on v1

--- a/solution.py
+++ b/solution.py
@@ -1,4 +1,5 @@
 import functools
+import math
 
 import jax
 import jax.numpy as jnp
@@ -13,7 +14,8 @@
 F32 = jnp.float32
 BF16 = jnp.bfloat16
 MESH = pl.DeviceIdType.MESH
-SPLITS = (2, 2, 2, 1, 1, 1)
+SPLITS = (2, 2, 2, 1, 1, 2)
+PIECE = 32
 
 
 def aligned(value, unit):
@@ -47,7 +49,12 @@
 def kernel(
     sizes,
     tokens,
-    gains,
+    gain0,
+    gain1,
+    gain2,
+    gain3,
+    gain4,
+    gain5,
     gate_w,
     up_w,
     down_w,
@@ -68,6 +75,8 @@
     hidden,
     mixed,
     parts,
+    paired,
+    outgoing,
     landed,
     streams,
     own_sem,
@@ -77,10 +86,16 @@
     right_recv,
     side_send,
     side_recv,
+    pair_send,
+    pair_recv,
     sum_send,
     sum_recv,
+    twin_send,
+    twin_recv,
     put_send,
     put_recv,
+    pass_send,
+    pass_recv,
     last_sem,
 ):
     grp_n, fs_n, tp_n = sizes
@@ -89,6 +104,14 @@
     fulls = (gate_full, up_full, down_full, u_full, v_full, out_full)
     count, width = tokens.shape
     chunk = count // tp_n
+    chips = tp_n // 2
+    chip, core = tp // 2, lax.rem(tp, 2)
+    twin = tp + 1 - 2 * core
+    columns = pair_send.shape[1]
+    column = width // columns
+    piece_n = put_send.shape[1]
+    piece_rows = chunk // piece_n
+    all_gains = (gain0, gain1, gain2, gain3, gain4, gain5)
 
     barrier = pltpu.get_barrier_semaphore()
     for move in (1, fs_n - 1):
@@ -256,31 +279,78 @@
 
             lax.fori_loop(0, fs_n, step, 0)
 
-    def sum_copy(phase, move):
-        peer = lax.rem(tp + move, tp_n)
-        rows = pl.ds(aligned(peer * chunk, 16), chunk)
-        return pltpu.make_async_remote_copy(
-            src_ref=parts.at[phase, rows, :],
-            dst_ref=landed.at[phase, move - 1],
-            send_sem=sum_send.at[phase, move - 1],
-            recv_sem=sum_recv.at[phase, move - 1],
-            device_id={"tp": peer},
-            device_id_type=MESH,
-        )
-
-    def put_copy(phase, move):
-        rows = pl.ds(aligned(tp * chunk, 16), chunk)
+    def other(move, which):
+        return lax.rem(chip + move, chips) * 2 + which
+
+    def origin(move, which):
+        return lax.rem(chip + chips - move, chips) * 2 + which
+
+    def chunk_rows(owner):
+        return pl.ds(aligned(owner * chunk, 16), chunk)
+
+    def column_span(col):
+        return pl.ds(aligned(col * column, 128), column)
+
+    def pair_copy(phase, col, move):
+        span = column_span(col)
+        return pltpu.make_async_remote_copy(
+            src_ref=parts.at[phase, chunk_rows(other(move, 1 - core)), span],
+            dst_ref=paired.at[phase, move, :, span],
+            send_sem=pair_send.at[phase, col, move],
+            recv_sem=pair_recv.at[phase, col, move],
+            device_id={"tp": twin},
+            device_id_type=MESH,
+        )
+
+    def sum_copy(phase, col, move):
+        span = column_span(col)
+        return pltpu.make_async_remote_copy(
+            src_ref=outgoing.at[phase, move, :, span],
+            dst_ref=landed.at[phase, move, :, span],
+            send_sem=sum_send.at[phase, col, move],
+            recv_sem=sum_recv.at[phase, col, move],
+            device_id={"tp": other(move, core)},
+            device_id_type=MESH,
+        )
+
+    def piece_span(owner, piece):
+        return pl.ds(aligned(owner * chunk + piece * piece_rows, 16), piece_rows)
+
+    def twin_copy(phase, piece):
+        rows = piece_span(tp, piece)
         return pltpu.make_async_remote_copy(
             src_ref=streams.at[phase, rows, :],
             dst_ref=streams.at[phase, rows, :],
-            send_sem=put_send.at[phase, move - 1],
-            recv_sem=put_recv.at[phase, move - 1],
-            device_id={"tp": lax.rem(tp + move, tp_n)},
+            send_sem=twin_send.at[phase, piece],
+            recv_sem=twin_recv.at[phase, piece],
+            device_id={"tp": twin},
+            device_id_type=MESH,
+        )
+
+    def put_copy(phase, piece, move):
+        rows = piece_span(tp, piece)
+        return pltpu.make_async_remote_copy(
+            src_ref=streams.at[phase, rows, :],
+            dst_ref=streams.at[phase, rows, :],
+            send_sem=put_send.at[phase, piece, move],
+            recv_sem=put_recv.at[phase, piece, move],
+            device_id={"tp": other(move, core)},
+            device_id_type=MESH,
+        )
+
+    def pass_copy(phase, piece, move):
+        rows = piece_span(origin(move, core), piece)
+        return pltpu.make_async_remote_copy(
+            src_ref=streams.at[phase, rows, :],
+            dst_ref=streams.at[phase, rows, :],
+            send_sem=pass_send.at[phase, piece, move],
+            recv_sem=pass_recv.at[phase, piece, move],
+            device_id={"tp": twin},
             device_id_type=MESH,
         )
 
     def gain(row):
-        return gains[row : row + 1, :].astype(F32)
+        return all_gains[row][...].astype(F32).reshape(1, width)
 
     def norm_rows(load, row):
         def body(low):
@@ -290,30 +360,58 @@
 
         over_rows(count, 32, body)
 
-    def start_sums(phase):
-        for move in range(1, tp_n):
-            sum_copy(phase, move).start()
+    def start_sums(phase, col):
+        for move in range(1, chips):
+            pair_copy(phase, col, move).wait_recv()
+            span = column_span(col)
+            mine = parts[phase, chunk_rows(other(move, core)), span].astype(F32)
+            both = mine + paired[phase, move, :, span].astype(F32)
+            outgoing[phase, move, :, span] = both.astype(BF16)
+            sum_copy(phase, col, move).start()
 
     def add_branch(phase, load, row, factor):
-        for move in range(1, tp_n):
-            sum_copy(phase, move).wait_recv()
-
-        def body(low):
-            rows = pl.ds(aligned(tp * chunk + low, 16), 16)
-            total = parts[phase, rows, :].astype(F32)
-            for move in range(1, tp_n):
-                total = total + landed[phase, move - 1, pl.ds(low, 16), :].astype(F32)
-            scale = lax.rsqrt(jnp.mean(total * total, axis=-1, keepdims=True) + 1e-06)
-            branch = total * scale * gain(row)
-            streams[phase, rows, :] = (load(rows).astype(F32) + factor * branch).astype(BF16)
-
-        over_rows(chunk, 16, body)
-        for move in range(1, tp_n):
-            put_copy(phase, move).start()
+        for col in range(columns):
+            pair_copy(phase, col, 0).wait_recv()
+            for move in range(1, chips):
+                sum_copy(phase, col, move).wait_recv()
+        for piece in range(piece_n):
+
+            def body(low, piece=piece):
+                here = pl.ds(aligned(piece * piece_rows + low, 16), 16)
+                rows = pl.ds(aligned(tp * chunk + piece * piece_rows + low, 16), 16)
+                total = parts[phase, rows, :].astype(F32) + paired[phase, 0, here, :].astype(F32)
+                for move in range(1, chips):
+                    total = total + landed[phase, move, here, :].astype(F32)
+                scale = lax.rsqrt(jnp.mean(total * total, axis=-1, keepdims=True) + 1e-06)
+                branch = total * scale * gain(row)
+                streams[phase, rows, :] = (load(rows).astype(F32) + factor * branch).astype(BF16)
+
+            over_rows(piece_rows, 16, body)
+            for move in range(1, chips):
+                put_copy(phase, piece, move).start()
+            twin_copy(phase, piece).start()
 
     def wait_put(phase):
-        for move in range(1, tp_n):
-            put_copy(phase, move).wait_recv()
+        for piece in range(piece_n):
+            for move in range(1, chips):
+                put_copy(phase, piece, move).wait_recv()
+                pass_copy(phase, piece, move).start()
+        for piece in range(piece_n):
+            twin_copy(phase, piece).wait_recv()
+            for move in range(1, chips):
+                pass_copy(phase, piece, move).wait_recv()
+
+    def finish_phase(phase):
+        for col in range(columns):
+            for move in range(chips):
+                pair_copy(phase, col, move).wait_send()
+            for move in range(1, chips):
+                sum_copy(phase, col, move).wait_send()
+        for piece in range(piece_n):
+            twin_copy(phase, piece).wait_send()
+            for move in range(1, chips):
+                put_copy(phase, piece, move).wait_send()
+                pass_copy(phase, piece, move).wait_send()
 
     def hidden_units():
         def body(low, size):
@@ -325,39 +423,46 @@
         over_tiles(hidden.shape[1], body)
 
     def project(phase, left, right):
-        size = right.shape[2]
-
-        def one(block, low):
-            terms = jnp.dot(left[...], right[block], preferred_element_type=F32)
-            parts[phase, :, pl.ds(low, size)] = terms.astype(BF16)
-
-        if size % 128 == 0:
-
-            def step(block, carry):
-                one(block, pl.multiple_of(block * size, 128))
-                return carry
-
-            lax.fori_loop(0, fs_n, step, 0)
-        else:
-            for block in range(fs_n):
-                one(block, block * size)
+        blocks = fs_n // columns
+
+        def step(col, carry):
+            terms = [
+                jnp.dot(left[...], right[col * blocks + b], preferred_element_type=F32)
+                for b in range(blocks)
+            ]
+            terms = terms[0] if blocks == 1 else jnp.concatenate(terms, axis=1)
+            parts[phase, :, column_span(col)] = terms.astype(BF16)
+            for move in range(chips - 1, -1, -1):
+                pair_copy(phase, col, move).start()
+
+            @pl.when(col > 0)
+            def _():
+                start_sums(phase, col - 1)
+
+            return carry
+
+        lax.fori_loop(0, columns, step, 0)
+        start_sums(phase, columns - 1)
 
     def mix():
         rows = lax.broadcasted_iota(jnp.int32, (BLOCK, BLOCK), 0)
         cols = lax.broadcasted_iota(jnp.int32, (BLOCK, BLOCK), 1)
+        all_spatial_gain = spatial_gain[...].astype(F32).reshape(1, mixed.shape[1])
         for g in range(mixed.shape[1] // GROUP_WIDTH):
             span = slice(g * GROUP_WIDTH, (g + 1) * GROUP_WIDTH)
             v = gelu(jnp.dot(normed[...], v_full[:, span], preferred_element_type=F32))
             u = gelu(jnp.dot(normed[...], u_full[:, span], preferred_element_type=F32))
             v = v - jnp.mean(v, axis=-1, keepdims=True)
             v = v * lax.rsqrt(jnp.mean(v * v, axis=-1, keepdims=True) + 1e-05)
-            v = (v * spatial_gain[:, span].astype(F32)).astype(BF16)
+            v = (v * all_spatial_gain[:, span]).astype(BF16)
             weight = spatial_weight[g].astype(F32)
             weight = jnp.where(rows >= cols, weight, 0.0).astype(BF16)
+            bias = spatial_bias[...][g : g + 1, :].astype(F32)
+            bias = jnp.sum(jnp.where(rows == cols, bias, 0.0), axis=1, keepdims=True)
             for n in range(count // BLOCK):
                 part = slice(n * BLOCK, (n + 1) * BLOCK)
                 spatial = jnp.dot(weight, v[part], preferred_element_type=F32)
-                spatial = spatial + spatial_bias[:, g : g + 1]
+                spatial = spatial + bias
                 mixed[part, span] = (u[part] * spatial).astype(BF16)
 
     load_tokens = lambda rows: tokens[rows, :]
@@ -370,48 +475,42 @@
         own_copy(w).start()
     norm_rows(load_tokens, 0)
 
-    def relay_weight(w):
-        for unit in range(len(units)):
-            if units[unit][0] == w:
-                relay(unit)
-                send_own(unit + 2)
-
-    relay_weight(0)
-    relay_weight(1)
+    for unit in range(5):
+        relay(unit)
+        send_own(unit + 2)
     wait_weight(0)
-    relay_weight(2)
     wait_weight(1)
     hidden_units()
+    relay(5)
+    send_own(7)
+    relay(6)
+    send_own(8)
+    send_own(9)
     wait_weight(2)
     project(0, hidden, down_full)
-    start_sums(0)
-    relay_weight(3)
+    relay(7)
     add_branch(0, load_tokens, 1, 0.5)
-    relay_weight(4)
+    relay(8)
     wait_put(0)
     norm_rows(load_first, 2)
-    relay_weight(5)
+    relay(9)
     wait_weight(3)
     wait_weight(4)
     mix()
     wait_weight(5)
     project(1, mixed, out_full)
-    start_sums(1)
     add_branch(1, load_first, 3, 1.0)
     wait_put(1)
     norm_rows(load_second, 4)
     hidden_units()
     project(2, hidden, down_full)
-    start_sums(2)
     add_branch(2, load_second, 5, 0.5)
     finish_sends()
     wait_put(2)
     last = pltpu.make_async_copy(streams.at[2], result, last_sem)
     last.start()
     for phase in range(3):
-        for move in range(1, tp_n):
-            sum_copy(phase, move).wait_send()
-            put_copy(phase, move).wait_send()
+        finish_phase(phase)
     last.wait()
 
 
@@ -438,9 +537,10 @@
     count, width = tokens.shape
     hidden_width = gate_weight.shape[1]
     channels = mix_u_weight.shape[1]
-    gains = jnp.stack(
-        [ffn_pre_gain, ffn_post_gain, mix_pre_gain, mix_post_gain, late_pre_gain, late_post_gain]
-    )
+    columns = math.gcd(fs_n, 4)
+    chips = tp_n // 2
+    chunk = count // tp_n
+    pieces = max(1, chunk // PIECE)
     vmem = pl.BlockSpec(memory_space=pltpu.VMEM)
     hbm = pl.BlockSpec(memory_space=pl.ANY)
     units = sum(SPLITS)
@@ -448,7 +548,7 @@
     return pl.pallas_call(
         functools.partial(kernel, sizes),
         out_shape=jax.ShapeDtypeStruct((count, width), BF16),
-        in_specs=[vmem, vmem, hbm, hbm, hbm, hbm, hbm, hbm, vmem, vmem, vmem],
+        in_specs=[vmem] * 7 + [hbm, hbm, hbm, hbm, hbm, hbm, vmem, vmem, vmem],
         out_specs=hbm,
         scratch_shapes=[
             pltpu.VMEM((width, hidden_width), BF16),
@@ -461,7 +561,9 @@
             pltpu.VMEM((count, hidden_width), BF16),
             pltpu.VMEM((count, channels), BF16),
             pltpu.VMEM((3, count, width), BF16),
-            pltpu.VMEM((3, tp_n - 1, count // tp_n, width), BF16),
+            pltpu.VMEM((3, chips, chunk, width), BF16),
+            pltpu.VMEM((3, chips, chunk, width), BF16),
+            pltpu.VMEM((3, chips, chunk, width), BF16),
             pltpu.VMEM((3, count, width), BF16),
             dma((6,)),
             dma((units, fs_n)),
@@ -470,10 +572,16 @@
             dma((units, fs_n)),
             dma((units, 2, grp_n - 1, fs_n)),
             dma((units, 2, grp_n - 1, fs_n)),
-            dma((3, tp_n - 1)),
-            dma((3, tp_n - 1)),
-            dma((3, tp_n - 1)),
-            dma((3, tp_n - 1)),
+            dma((3, columns, chips)),
+            dma((3, columns, chips)),
+            dma((3, columns, chips)),
+            dma((3, columns, chips)),
+            dma((3, pieces)),
+            dma((3, pieces)),
+            dma((3, pieces, chips)),
+            dma((3, pieces, chips)),
+            dma((3, pieces, chips)),
+            dma((3, pieces, chips)),
             dma(()),
         ],
         compiler_params=pltpu.CompilerParams(
@@ -481,16 +589,21 @@
         ),
     )(
         tokens,
-        gains,
+        ffn_pre_gain,
+        ffn_post_gain,
+        mix_pre_gain,
+        mix_post_gain,
+        late_pre_gain,
+        late_post_gain,
         gate_weight,
         up_weight,
         down_weight,
         mix_u_weight,
         mix_v_weight,
         mix_out_weight,
-        spatial_gain.reshape(1, channels),
+        spatial_gain,
         spatial_weight,
-        spatial_bias.astype(F32).T,
+        spatial_bias,
     )
 
 

time: 283 us -> 263 us (0.929)
  Pallas kernels: 273 us -> 260 us
  local copies, waits for them, and re-layouts: 9.8 us -> 2.3 us
    pallas_call x1, Pallas kernels: 273 us -> 260 us  [shards(): pl.pallas_call(functools.partial(kernel, sizes), out_shape=jax.ShapeDtype...]
    another operation x7 -> x0, local copies, waits for them, and re-layouts: 4.83 us -> none  [shards(): jnp.stack([ffn_pre_gain, ffn_post_gain, mix_pre_gain, mix_post_gain, late...]
where the time goes in v2:
time: 263 us
  Pallas kernels  260 us (99%)
    pallas_call x1, Pallas kernels, shards(): pl.pallas_call(functools.partial(kernel, sizes), out_shape=jax.ShapeDtype...  260 us

profile of v2, /device:TPU:1, one launch (start us, length us, event | category | flops | bytes accessed | tf_op | source)
XLA Modules:
  0.0 262.6 jit_solution(7998717207873491789)
XLA Ops:
  0.0 260.3 %shard_map.154 = bf16[256,2048]{1,0:T(8,128)(2,1)} custom-call(bf16[256,2048]{1,0:T(8,128)(2,1)} %tokens.1, bf16[2048]{0:T(1024)(128)(2,1)} %gain0.1, bf16[2048]{0:T(1024)(128)(2,1)} %gain1.1, bf16[2048]{0:T(1024)(128)(2,1)} %gain2.1, bf16[2048]{0:T(1024)(128)(2,1)} %gain3.1, bf16[2048]{0:T(1024)(128)(2,1)} %gain4.1, bf16[2048]{0:T(1024)(128)(2,1)} %gain5.1, ...), custom_call_target="tpu_custom_call" | custom-call | tf_op jit(solution)/shard_map/pallas_call | solution.py:548
  260.3 2.3 copy.18

commit v3 on v2

--- a/solution.py
+++ b/solution.py
@@ -22,15 +22,15 @@
     return value if isinstance(value, int) else pl.multiple_of(value, unit)
 
 
-def over_tiles(width, body):
+def over_tiles(width, body, third, thirds):
     count = width // TILE
 
     def step(i, carry):
         body(pl.multiple_of(i * TILE, TILE), TILE)
         return carry
 
-    lax.fori_loop(0, count, step, 0)
-    if width % TILE:
+    lax.fori_loop(count * third // thirds, count * (third + 1) // thirds, step, 0)
+    if width % TILE and third == thirds - 1:
         body(count * TILE, width % TILE)
 
 
@@ -203,7 +203,7 @@
         def _():
             to_left(unit, 0, own=True).start()
 
-    def relay(unit):
+    def relay(unit, low=1, high=fs_n):
         def step(hop, carry):
             @pl.when(fs >= hop)
             def _():
@@ -229,7 +229,7 @@
 
             return carry
 
-        lax.fori_loop(1, fs_n, step, 0)
+        lax.fori_loop(low, high, step, 0)
 
     def wait_weight(w):
         own_copy(w).wait()
@@ -413,14 +413,14 @@
                 put_copy(phase, piece, move).wait_send()
                 pass_copy(phase, piece, move).wait_send()
 
-    def hidden_units():
+    def hidden_units(third=0, thirds=1):
         def body(low, size):
             cols = pl.ds(low, size)
             gate = jnp.dot(normed[...], gate_full[:, cols], preferred_element_type=F32)
             upper = jnp.dot(normed[...], up_full[:, cols], preferred_element_type=F32)
             hidden[:, cols] = (gate / (1.0 + jnp.exp(-gate)) * upper).astype(BF16)
 
-        over_tiles(hidden.shape[1], body)
+        over_tiles(hidden.shape[1], body, third, thirds)
 
     def project(phase, left, right):
         blocks = fs_n // columns
@@ -480,8 +480,9 @@
         send_own(unit + 2)
     wait_weight(0)
     wait_weight(1)
-    hidden_units()
-    relay(5)
+    for third in range(3):
+        hidden_units(third, 3)
+        relay(5, min(1 + third, fs_n), fs_n if third == 2 else min(2 + third, fs_n))
     send_own(7)
     relay(6)
     send_own(8)

time: 263 us -> 263 us (level)
  no operation moved by 1% of the time
where the time goes in v3:
time: 263 us
  Pallas kernels  260 us (99%)
    pallas_call x1, Pallas kernels, shards(): pl.pallas_call(functools.partial(kernel, sizes), out_shape=jax.ShapeDtype...  260 us

profile of v3, /device:TPU:1, one launch (start us, length us, event | category | flops | bytes accessed | tf_op | source)
XLA Modules:
  0.0 262.6 jit_solution(11517721658453160482)
XLA Ops:
  0.0 260.3 %shard_map.154 = bf16[256,2048]{1,0:T(8,128)(2,1)} custom-call(bf16[256,2048]{1,0:T(8,128)(2,1)} %tokens.1, bf16[2048]{0:T(1024)(128)(2,1)} %gain0.1, bf16[2048]{0:T(1024)(128)(2,1)} %gain1.1, bf16[2048]{0:T(1024)(128)(2,1)} %gain2.1, bf16[2048]{0:T(1024)(128)(2,1)} %gain3.1, bf16[2048]{0:T(1024)(128)(2,1)} %gain4.1, bf16[2048]{0:T(1024)(128)(2,1)} %gain5.1, ...), custom_call_target="tpu_custom_call" | custom-call | tf_op jit(solution)/shard_map/pallas_call | solution.py:549
  260.3 2.3 copy.18
